TPU v7x, 256 devices: a whole 4x4x8 slice. The times are simulated.
256 devices in a mesh: fs: 32 (over z, x), tp: 8 (over y, core).
Axes of the slice: x: 4, y: 4, z: 8, core: 2. Of those that a mesh axis runs over, the one named last changes fastest.
Arguments:
- saved_input: bfloat16 [81920, 2048], P('fs'), may hold values from -6 to 6
- value_cot: bfloat16 [81920, 1024], P('fs', 'tp'), may hold values from -6 to 6
- query_cot: bfloat16 [81920, 512], P('fs', 'tp'), may hold values from -6 to 6
- value_master: float32 [2048, 1024], P('fs', 'tp'), may hold values from -0.125 to 0.125
- query_master: float32 [2048, 512], P('fs', 'tp'), may hold values from -0.125 to 0.125
- value_factor: bfloat16 [2048, 256], P('fs'), may hold values from -0.125 to 0.125
- query_factor: bfloat16 [2048, 256], P('fs'), may hold values from -0.125 to 0.125
- value_first: float32 [256, 1024], P('fs', 'tp'), as said below
- value_second: float32 [256, 1024], P('fs', 'tp'), as said below
- query_first: float32 [256, 512], P('fs', 'tp'), as said below
- query_second: float32 [256, 512], P('fs', 'tp'), as said below
Outputs:
- value_step: float32 [2048, 1024], P('fs', 'tp')
- query_step: float32 [2048, 512], P('fs', 'tp')
- value_master_new: float32 [2048, 1024], P('fs', 'tp')
- query_master_new: float32 [2048, 512], P('fs', 'tp')
- value_copy: bfloat16 [2048, 1024], P(None, 'tp')
- query_copy: bfloat16 [2048, 512], P(None, 'tp')
- value_first_new: float32 [256, 1024], P('fs', 'tp')
- value_second_new: float32 [256, 1024], P('fs', 'tp')
- query_first_new: float32 [256, 512], P('fs', 'tp')
- query_second_new: float32 [256, 512], P('fs', 'tp')
Inputs may be any that keep to these rules, and one draw needn't show every extreme that they name: `value_first`: first moments are real-valued of the projected gradient's order. `value_second`: second moments are positive. `query_first`: first moments are real-valued of the projected gradient's order. `query_second`: second moments are positive.
All inputs are finite; a program needn't handle non-finite values.
Results may differ from a plain program's by a relative error of at most 0.001.
Values may be sent and summed in bfloat16 or wider, within the bound.
A program may use at most 64 MiB of HBM per device.

v0:
```python
import jax
import jax.numpy as jnp
from jax import lax
from jax.sharding import Mesh
from jax.sharding import PartitionSpec as P

RANK = 256
V_W = 1024
QK_W = 512
FS = ("fs_0", "fs_1")
FS_TP = ("fs_0", "fs_1", "tp_0", "tp_1")
TP = ("tp_0", "tp_1")
BETA_ONE = 0.9
BETA_TWO = 0.95
DENOM_EPS = 1e-08
NORM_EPS = 1e-06
STEP_SIZE = 0.05


def split_up(x, dim, size):
    dims = x.shape
    blocks = x.reshape(*dims[:dim], size, dims[dim] // size, *dims[dim + 1 :])
    return jnp.moveaxis(blocks, dim, 0)


def sent_and_summed(x, axis, dim):
    blocks = split_up(x, dim, lax.axis_size(axis))
    arrived = lax.all_to_all(blocks, axis, split_axis=0, concat_axis=0, tiled=True)
    return arrived.sum(axis=0)


def sent_together(arrays, axis, dim, along):
    ends, at = ([], 0)
    for a in arrays[:-1]:
        at += a.shape[along]
        ends.append(at)
    both = jnp.concatenate(arrays, axis=along)
    return tuple(jnp.split(sent_and_summed(both, axis, dim), ends, axis=along))


def sent_together_2(arrays, axis, dim, along):
    both = jnp.concatenate(arrays, axis=along)
    out, at, outs = (lax.all_gather(both, axis, axis=dim, tiled=True), 0, [])
    for a in arrays:
        outs.append(lax.slice_in_dim(out, at, at + a.shape[along], axis=along))
        at += a.shape[along]
    return tuple(outs)


def by_axis(x, axes):
    for axis in axes:
        x = lax.psum(x, axis)
    return x


def moment_update(projected, first, second):
    first_new = BETA_ONE * first + (1.0 - BETA_ONE) * projected
    second_new = BETA_TWO * second + (1.0 - BETA_TWO) * projected * projected
    direction = first_new / (jnp.sqrt(second_new) + DENOM_EPS)
    return (first_new, second_new, direction)


def token_product(left, right):
    return lax.dot_general(
        left, right, (((0,), (0,)), ((), ())), preferred_element_type=jnp.float32
    )


def on_device(
    saved_input,
    value_cot,
    query_cot,
    value_master,
    query_master,
    value_factor,
    query_factor,
    value_first,
    value_second,
    query_first,
    query_second,
):
    shards = lax.axis_size(FS)
    tokens_all = saved_input.shape[0] * shards
    highest = lax.Precision.HIGHEST
    columns = saved_input
    value_grad = sent_and_summed(token_product(columns, value_cot), FS, 0) / tokens_all
    columns = saved_input
    query_grad = sent_and_summed(token_product(columns, query_cot), FS, 0) / tokens_all
    value_part = jnp.dot(value_factor.astype(jnp.float32).T, value_grad, precision=highest)
    query_part = jnp.dot(query_factor.astype(jnp.float32).T, query_grad, precision=highest)
    value_share, query_share = sent_together((value_part, query_part), FS, 0, 1)
    value_first_new, value_second_new, value_dir_own = moment_update(
        value_share, value_first, value_second
    )
    query_first_new, query_second_new, query_dir_own = moment_update(
        query_share, query_first, query_second
    )
    value_direction, query_direction = sent_together_2((value_dir_own, query_dir_own), FS, 0, 1)
    square_sum = by_axis(
        jnp.sum(value_dir_own * value_dir_own) + jnp.sum(query_dir_own * query_dir_own), FS_TP
    )
    update_scale = 1.0 / jnp.sqrt(square_sum / (RANK * (V_W + QK_W)) + NORM_EPS)
    value_step = (
        jnp.dot(value_factor.astype(jnp.float32), value_direction, precision=highest) * update_scale
    )
    query_step = (
        jnp.dot(query_factor.astype(jnp.float32), query_direction, precision=highest) * update_scale
    )
    value_master_new = value_master - STEP_SIZE * value_step
    query_master_new = query_master - STEP_SIZE * query_step
    value_copy, query_copy = sent_together_2(
        (value_master_new.astype(jnp.bfloat16), query_master_new.astype(jnp.bfloat16)), FS, 0, 1
    )
    return (
        value_step,
        query_step,
        value_master_new,
        query_master_new,
        value_copy,
        query_copy,
        value_first_new,
        value_second_new,
        query_first_new,
        query_second_new,
    )


def solution(mesh):
    split = Mesh(mesh.devices.reshape(8, 4, 4, 2), ("fs_0", "fs_1", "tp_0", "tp_1"))
    placed = (
        P(FS, None),
        P(FS, TP),
        P(FS, TP),
        P(FS, TP),
        P(FS, TP),
        P(FS, None),
        P(FS, None),
        P(FS, TP),
        P(FS, TP),
        P(FS, TP),
        P(FS, TP),
    )
    return jax.shard_map(
        on_device,
        mesh=split,
        in_specs=placed,
        out_specs=(
            P(FS, TP),
            P(FS, TP),
            P(FS, TP),
            P(FS, TP),
            P(None, TP),
            P(None, TP),
            P(FS, TP),
            P(FS, TP),
            P(FS, TP),
            P(FS, TP),
        ),
        check_vma=False,
    )
```

profile of v0, /device:TPU:2, one launch (start us, length us, event | category | flops | bytes accessed | tf_op | source)
XLA Modules:
  0.0 230.8 jit_solution(3035166584856945840)
XLA Ops:
  0.6 0.0 copy-start
  0.7 6.1 %fusion.17 = f32[2048,64]{0,1:T(8,128)S(1)} fusion(bf16[2560,64]{0,1:T(8,128)(2,1)} %param.13, bf16[2560,2048]{1,0:T(8,128)(2,1)} %param.11), kind=kOutput, calls=%fused_computation.34 | convolution fusion | flops 671088640 | bytes 11337728 | tf_op jit(solution)/shard_map/dot_general | solution.py:64
  6.7 0.4 reshape.30
  7.2 0.6 copy.30
  7.8 1.4 reshape.32
  9.2 11.7 %all-to-all-start.1 = ((f32[32,1,4096]{2,1,0:T(1,128)}), f32[32,1,4096]{2,1,0:T(1,128)S(1)}, u32[]{:S(2)}, u32[]{:S(2)}) async-start(f32[32,1,4096]{2,1,0:T(1,128)} %reshape.32), calls=%async_computation.1 | async-start | bytes 1048576 | tf_op jit(solution)/shard_map/all_to_all | solution.py:28
  21.0 0.0 copy-start.7
  21.1 7.9 %fusion.16 = f32[2048,128]{1,0:T(8,128)} fusion(bf16[2560,2048]{1,0:T(8,128)(2,1)} %param.11, bf16[2560,128]{1,0:T(8,128)(2,1)S(1)} %copy-done), kind=kOutput, calls=%fused_computation.33 | convolution fusion | flops 1342177280 | bytes 12189696 | tf_op jit(solution)/shard_map/dot_general | solution.py:64
  29.0 8.8 %all-to-all-done.1 = f32[32,1,4096]{2,1,0:T(1,128)S(1)} async-done(((f32[32,1,4096]{2,1,0:T(1,128)}), f32[32,1,4096]{2,1,0:T(1,128)S(1)}, u32[]{:S(2)}, u32[]{:S(2)}) %all-to-all-start.1) | async-done | bytes 524320 | tf_op jit(solution)/shard_map/all_to_all | solution.py:28
  37.8 5.6 %all-to-all-start = ((f32[32,64,128]{2,1,0:T(8,128)}), f32[32,64,128]{2,1,0:T(8,128)S(1)}, u32[]{:S(2)}, u32[]{:S(2)}) async-start(f32[32,64,128]{2,1,0:T(8,128)} %bitcast), calls=%async_computation | async-start | bytes 2097152 | tf_op jit(solution)/shard_map/all_to_all | solution.py:28
  43.4 0.5 broadcast.6
  43.9 1.9 reduce
  45.8 0.4 reshape.33
  46.2 0.1 bitcast_reduce_fusion
  46.3 0.2 convolution_bitcast_fusion.1
  46.5 24.1 %all-to-all-done = f32[32,64,128]{2,1,0:T(8,128)S(1)} async-done(((f32[32,64,128]{2,1,0:T(8,128)}), f32[32,64,128]{2,1,0:T(8,128)S(1)}, u32[]{:S(2)}, u32[]{:S(2)}) %all-to-all-start) | async-done | bytes 1048608 | tf_op jit(solution)/shard_map/all_to_all | solution.py:28
  70.6 0.1 reduce_sum.45
  70.7 0.3 convolution_bitcast_fusion
  71.0 0.1 copy.26
  71.1 15.3 %all_to_all.15 = f32[32,8,192]{2,1,0:T(8,128)S(1)} all-to-all(f32[32,8,192]{2,1,0:T(8,128)S(1)} %bitcast.26), channel_id=1, replica_groups=mesh['fs_0'=8,'fs_1'=4,'tp_0'=4,'tp_1'=2] {'fs_0','fs_1'}, dimensions={0} | all-to-all | bytes 393216 | tf_op jit(solution)/shard_map/all_to_all | solution.py:28
  86.5 1.2 multiply_reduce_fusion
  87.7 1.2 multiply_reduce_fusion.1
  90.2 16.0 %psum.28 = f32[]{:T(128)} all-reduce(f32[]{:T(128)S(6)} %add.46), channel_id=1, replica_groups=mesh['fs_0'=8,'fs_1'=4,'tp_0'=4,'tp_1'=2] {'fs_0'}, use_global_device_ids=true, to_apply=%region_5.0 | all-reduce | flops 1 | bytes 8 | tf_op jit(solution)/shard_map/psum | solution.py:52
  106.2 10.0 %psum.29 = f32[]{:T(128)} all-reduce(f32[]{:T(128)} %psum.28), channel_id=1, replica_groups=mesh['fs_0'=8,'fs_1'=4,'tp_0'=4,'tp_1'=2] {'fs_1'}, use_global_device_ids=true, to_apply=%region_6.0 | all-reduce | flops 1 | bytes 8 | tf_op jit(solution)/shard_map/psum | solution.py:52
  116.2 11.3 %psum.30 = f32[]{:T(128)} all-reduce(f32[]{:T(128)} %psum.29), channel_id=1, replica_groups=mesh['fs_0'=8,'fs_1'=4,'tp_0'=4,'tp_1'=2] {'tp_0'}, use_global_device_ids=true, to_apply=%region_7.0 | all-reduce | flops 1 | bytes 8 | tf_op jit(solution)/shard_map/psum | solution.py:52
  127.5 47.2 %all_gather.6 = f32[256,192]{1,0:T(8,128)S(1)} all-gather(f32[8,192]{1,0:T(8,128)S(1)} %pad_maximum_fusion.2), channel_id=1, replica_groups=mesh['fs_0'=8,'fs_1'=4,'tp_0'=4,'tp_1'=2] {'fs_0','fs_1'}, dimensions={0}, use_global_device_ids=true | all-gather | bytes 202752 | tf_op jit(solution)/shard_map/all_gather | solution.py:43
  174.8 3.1 %psum.31 = f32[]{:T(128)} all-reduce(f32[]{:T(128)} %psum.30), channel_id=1, replica_groups=mesh['fs_0'=8,'fs_1'=4,'tp_0'=4,'tp_1'=2] {'tp_1'}, use_global_device_ids=true, to_apply=%region_8.0 | all-reduce | flops 1 | bytes 8 | tf_op jit(solution)/shard_map/psum | solution.py:52
  178.6 0.8 fusion.13
  179.4 0.8 fusion.12
  180.2 48.9 %all_gather.7 = bf16[2048,192]{1,0:T(8,128)(2,1)S(1)} all-gather(bf16[64,192]{1,0:T(8,128)(2,1)S(1)} %pad_maximum_fusion.1), channel_id=1, replica_groups=mesh['fs_0'=8,'fs_1'=4,'tp_0'=4,'tp_1'=2] {'fs_0','fs_1'}, dimensions={0}, use_global_device_ids=true | all-gather | bytes 811008 | tf_op jit(solution)/shard_map/all_gather | solution.py:43
  229.1 0.8 slice.18
  229.9 0.9 copy.27
  (21 shorter events, 0.1 us)
Async XLA Ops:
  0.6 20.4 %copy-start = (bf16[2560,128]{1,0:T(8,128)(2,1)S(1)}, bf16[2560,128]{1,0:T(8,128)(2,1)}, u32[]{:S(2)}) copy-start(bf16[2560,128]{1,0:T(8,128)(2,1)} %param.12) | copy-start | bytes 1966084
  7.8 38.5 %copy-start.1 = (bf16[64,256]{1,0:T(8,128)(2,1)S(1)}, bf16[64,256]{1,0:T(8,128)(2,1)}, u32[]{:S(2)}) copy-start(bf16[64,256]{1,0:T(8,128)(2,1)} %param.17) | copy-start | bytes 98308
  9.2 61.4 %copy-start.2 = (bf16[64,256]{1,0:T(8,128)(2,1)S(1)}, bf16[64,256]{1,0:T(8,128)(2,1)}, u32[]{:S(2)}) copy-start(bf16[64,256]{1,0:T(8,128)(2,1)} %param.16) | copy-start | bytes 98308
  9.2 28.6 %all-to-all-start.1 = ((f32[32,1,4096]{2,1,0:T(1,128)}), f32[32,1,4096]{2,1,0:T(1,128)S(1)}, u32[]{:S(2)}, u32[]{:S(2)}) async-start(f32[32,1,4096]{2,1,0:T(1,128)} %reshape.32), calls=%async_computation.1 | async-start | bytes 1048576 | tf_op jit(solution)/shard_map/all_to_all | solution.py:28
  21.0 65.5 %copy-start.5 = (f32[8,64]{1,0:T(8,128)S(1)}, f32[8,64]{1,0:T(8,128)}, u32[]{:S(2)}) copy-start(f32[8,64]{1,0:T(8,128)} %param.21) | copy-start | bytes 6148
  21.0 65.4 %copy-start.6 = (f32[8,64]{1,0:T(8,128)S(1)}, f32[8,64]{1,0:T(8,128)}, u32[]{:S(2)}) copy-start(f32[8,64]{1,0:T(8,128)} %param.20) | copy-start | bytes 6148
  21.0 66.6 %copy-start.7 = (f32[8,128]{1,0:T(8,128)S(1)}, f32[8,128]{1,0:T(8,128)}, u32[]{:S(2)}) copy-start(f32[8,128]{1,0:T(8,128)} %param.19) | copy-start | bytes 12292
  21.0 66.6 %copy-start.8 = (f32[8,128]{1,0:T(8,128)S(1)}, f32[8,128]{1,0:T(8,128)}, u32[]{:S(2)}) copy-start(f32[8,128]{1,0:T(8,128)} %param.18) | copy-start | bytes 12292
  21.1 157.5 %copy-start.3 = (f32[64,64]{1,0:T(8,128)S(1)}, f32[64,64]{1,0:T(8,128)}, u32[]{:S(2)}) copy-start(f32[64,64]{1,0:T(8,128)} %param.15) | copy-start | bytes 49156
  21.1 158.3 %copy-start.4 = (f32[64,128]{1,0:T(8,128)S(1)}, f32[64,128]{1,0:T(8,128)}, u32[]{:S(2)}) copy-start(f32[64,128]{1,0:T(8,128)} %param.14) | copy-start | bytes 98308
  37.8 32.8 %all-to-all-start = ((f32[32,64,128]{2,1,0:T(8,128)}), f32[32,64,128]{2,1,0:T(8,128)S(1)}, u32[]{:S(2)}, u32[]{:S(2)}) async-start(f32[32,64,128]{2,1,0:T(8,128)} %bitcast), calls=%async_computation | async-start | bytes 2097152 | tf_op jit(solution)/shard_map/all_to_all | solution.py:28
where the time goes:
time: 231 us
  blocking collectives  152 us (66%)
  waiting for transfers between devices  32.9 us (14%)
  starting transfers between devices  17.3 us (7%)
  matrix products  16.1 us (7%)
  local copies, waits for them, and re-layouts  5.34 us (2%)
  other arithmetic  4.52 us (2%)
  between operations  2.85 us (1%)
    all_gather x2, blocking collectives, sent_together_2(): out, at, outs = (lax.all_gather(both, axis, axis=dim, tiled=True), 0, [])  96.1 us
    psum x4, blocking collectives, by_axis(): x = lax.psum(x, axis)  40.4 us
    all_to_all x2, waiting for transfers between devices, sent_and_summed(): lax.all_to_all(blocks, axis, split_axis=0, concat_axis=0, tiled=True)  32.9 us
    all_to_all x2, starting transfers between devices, sent_and_summed(): lax.all_to_all(blocks, axis, split_axis=0, concat_axis=0, tiled=True)  17.3 us
    all_to_all x1, blocking collectives, sent_and_summed(): lax.all_to_all(blocks, axis, split_axis=0, concat_axis=0, tiled=True)  15.3 us
    dot_general x2, matrix products, token_product(): lax.dot_general(left, right, (((0,), (0,)), ((), ())), preferred_element_...  14 us
  transfers between devices with their start and end apart: 2, of which 2 were waited for; matrix products, arithmetic and copies ran while one was open for 5% of the time, Pallas kernels for 0%

commit v1 on v0

--- a/solution.py
+++ b/solution.py
@@ -49,7 +49,7 @@
 
 def by_axis(x, axes):
     for axis in axes:
-        x = lax.psum(x, axis)
+        x = jnp.sum(lax.all_gather(x, axis), axis=0)
     return x
 
 

time: 231 us -> 239 us (1.035)
  blocking collectives: 152 us -> 134 us
  waiting for transfers between devices: 32.9 us -> 42.2 us
  local copies, waits for them, and re-layouts: 5.34 us -> 13.4 us
  starting transfers between devices: 17.3 us -> 22.9 us
  other arithmetic: 4.52 us -> 6.93 us
    psum x4 -> x0, blocking collectives: 40.4 us -> none  [by_axis(): x = lax.psum(x, axis)]
    unnamed x0 -> x4, blocking collectives: none -> 38 us
    all_to_all x1 -> x0, blocking collectives: 15.3 us -> none  [sent_and_summed(): lax.all_to_all(blocks, axis, split_axis=0, concat_axis=0, tiled=True)]
    all_to_all x2 -> x3, waiting for transfers between devices: 32.9 us -> 42.2 us  [sent_and_summed(): lax.all_to_all(blocks, axis, split_axis=0, concat_axis=0, tiled=True)]
    unnamed x21 -> x41, local copies, waits for them, and re-layouts: 2.81 us -> 10.1 us
    all_to_all x2 -> x3, starting transfers between devices: 17.3 us -> 22.9 us  [sent_and_summed(): lax.all_to_all(blocks, axis, split_axis=0, concat_axis=0, tiled=True)]
    reduce_sum x0 -> x4, other arithmetic: none -> 2.41 us  [by_axis(): x = jnp.sum(lax.all_gather(x, axis), axis=0)]
  transfers between devices with their start and end apart: 2 -> 3, of which waited for: 2 -> 3; matrix products, arithmetic and copies ran while one was open for 5% -> 5% of each run, Pallas kernels for 0% -> 0%
where the time goes in v1:
time: 239 us; the launch traced here: 238 us
  blocking collectives  134 us (56%)
  waiting for transfers between devices  42.2 us (18%)
  starting transfers between devices  22.9 us (10%)
  matrix products  16.1 us (7%)
  local copies, waits for them, and re-layouts  13.4 us (6%)
  other arithmetic  6.93 us (3%)
  between operations  2.91 us (1%)
    all_gather x2, blocking collectives, sent_together_2(): out, at, outs = (lax.all_gather(both, axis, axis=dim, tiled=True), 0, [])  96 us
    all_to_all x3, waiting for transfers between devices, sent_and_summed(): lax.all_to_all(blocks, axis, split_axis=0, concat_axis=0, tiled=True)  42.2 us
    unnamed x4, blocking collectives  38 us
    all_to_all x3, starting transfers between devices, sent_and_summed(): lax.all_to_all(blocks, axis, split_axis=0, concat_axis=0, tiled=True)  22.9 us
    dot_general x2, matrix products, token_product(): lax.dot_general(left, right, (((0,), (0,)), ((), ())), preferred_element_...  14 us
    unnamed x41, local copies, waits for them, and re-layouts  10.1 us
  transfers between devices with their start and end apart: 3, of which 3 were waited for; matrix products, arithmetic and copies ran while one was open for 5% of the time, Pallas kernels for 0%

profile of v1, /device:TPU:2, one launch (start us, length us, event | category | flops | bytes accessed | tf_op | source)
XLA Modules:
  0.0 238.3 jit_solution(152003307422342132)
XLA Ops:
  0.7 6.1 %fusion.17 = f32[2048,64]{0,1:T(8,128)S(1)} fusion(bf16[2560,64]{0,1:T(8,128)(2,1)} %param.13, bf16[2560,2048]{1,0:T(8,128)(2,1)} %param.11), kind=kOutput, calls=%fused_computation.34 | convolution fusion | flops 671088640 | bytes 11337728 | tf_op jit(solution)/shard_map/dot_general | solution.py:64
  7.2 0.6 copy.30
  7.8 1.4 reshape.52
  9.2 11.7 %all-to-all-start.1 = ((f32[32,1,4096]{2,1,0:T(1,128)}), f32[32,1,4096]{2,1,0:T(1,128)S(1)}, u32[]{:S(2)}, u32[]{:S(2)}) async-start(f32[32,1,4096]{2,1,0:T(1,128)} %reshape.52), calls=%async_computation.1 | async-start | bytes 1048576 | tf_op jit(solution)/shard_map/all_to_all | solution.py:28
  21.1 7.9 %fusion.16 = f32[2048,128]{1,0:T(8,128)} fusion(bf16[2560,2048]{1,0:T(8,128)(2,1)} %param.11, bf16[2560,128]{1,0:T(8,128)(2,1)S(1)} %copy-done), kind=kOutput, calls=%fused_computation.33 | convolution fusion | flops 1342177280 | bytes 12189696 | tf_op jit(solution)/shard_map/dot_general | solution.py:64
  29.1 8.8 %all-to-all-done.1 = f32[32,1,4096]{2,1,0:T(1,128)S(1)} async-done(((f32[32,1,4096]{2,1,0:T(1,128)}), f32[32,1,4096]{2,1,0:T(1,128)S(1)}, u32[]{:S(2)}, u32[]{:S(2)}) %all-to-all-start.1) | async-done | bytes 524320 | tf_op jit(solution)/shard_map/all_to_all | solution.py:28
  37.8 5.6 %all-to-all-start = ((f32[32,64,128]{2,1,0:T(8,128)}), f32[32,64,128]{2,1,0:T(8,128)S(1)}, u32[]{:S(2)}, u32[]{:S(2)}) async-start(f32[32,64,128]{2,1,0:T(8,128)} %bitcast), calls=%async_computation | async-start | bytes 2097152 | tf_op jit(solution)/shard_map/all_to_all | solution.py:28
  43.9 1.9 reduce.4
  46.5 24.1 %all-to-all-done = f32[32,64,128]{2,1,0:T(8,128)S(1)} async-done(((f32[32,64,128]{2,1,0:T(8,128)}), f32[32,64,128]{2,1,0:T(8,128)S(1)}, u32[]{:S(2)}, u32[]{:S(2)}) %all-to-all-start) | async-done | bytes 1048608 | tf_op jit(solution)/shard_map/all_to_all | solution.py:28
  71.0 0.8 copy.26
  71.8 5.6 %all-to-all-start.2 = ((f32[32,8,192]{2,1,0:T(8,128)}), f32[32,8,192]{2,1,0:T(8,128)S(1)}, u32[]{:S(2)}, u32[]{:S(2)}) async-start(f32[32,8,192]{2,1,0:T(8,128)} %bitcast.3), calls=%async_computation.2 | async-start | bytes 524288 | tf_op jit(solution)/shard_map/all_to_all | solution.py:28
  78.0 9.3 %all-to-all-done.2 = f32[32,8,192]{2,1,0:T(8,128)S(1)} async-done(((f32[32,8,192]{2,1,0:T(8,128)}), f32[32,8,192]{2,1,0:T(8,128)S(1)}, u32[]{:S(2)}, u32[]{:S(2)}) %all-to-all-start.2) | async-done | bytes 196640 | tf_op jit(solution)/shard_map/all_to_all | solution.py:28
  87.4 1.2 multiply_reduce_fusion
  88.6 1.2 multiply_reduce_fusion.1
  91.1 0.8 dynamic-update-slice
  92.4 15.5 %all-reduce = f32[8]{0:T(128)S(1)} all-reduce(f32[8]{0:T(128)S(1)} %dynamic-update-slice), channel_id=1, replica_groups=mesh['fs_0'=8,'fs_1'=4,'tp_0'=4,'tp_1'=2] {'fs_0'}, use_global_device_ids=true, to_apply=%add | all-reduce | flops 8 | bytes 64
  107.9 0.6 reduce_sum.86
  108.5 1.4 dynamic-update-slice.1
  110.5 9.4 %all-reduce.1 = f32[4]{0:T(128)S(1)} all-reduce(f32[4]{0:T(128)S(1)} %dynamic-update-slice.1), channel_id=1, replica_groups=mesh['fs_0'=8,'fs_1'=4,'tp_0'=4,'tp_1'=2] {'fs_1'}, use_global_device_ids=true, to_apply=%add.1 | all-reduce | flops 4 | bytes 32
  119.9 0.6 reduce_sum.87
  120.5 1.4 dynamic-update-slice.2
  122.5 10.7 %all-reduce.2 = f32[4]{0:T(128)S(1)} all-reduce(f32[4]{0:T(128)S(1)} %dynamic-update-slice.2), channel_id=1, replica_groups=mesh['fs_0'=8,'fs_1'=4,'tp_0'=4,'tp_1'=2] {'tp_0'}, use_global_device_ids=true, to_apply=%add.2 | all-reduce | flops 4 | bytes 32
  133.2 0.6 reduce_sum.88
  133.8 1.4 dynamic-update-slice.3
  135.2 2.4 %all-reduce.3 = f32[2]{0:T(128)S(1)} all-reduce(f32[2]{0:T(128)S(1)} %dynamic-update-slice.3), channel_id=1, replica_groups=mesh['fs_0'=8,'fs_1'=4,'tp_0'=4,'tp_1'=2] {'tp_1'}, use_global_device_ids=true, to_apply=%add.3 | all-reduce | flops 2 | bytes 16
  137.6 0.6 reduce_sum.89
  138.9 47.3 %all_gather.30 = f32[256,192]{1,0:T(8,128)S(1)} all-gather(f32[8,192]{1,0:T(8,128)S(1)} %pad_maximum_fusion.2), channel_id=1, replica_groups=mesh['fs_0'=8,'fs_1'=4,'tp_0'=4,'tp_1'=2] {'fs_0','fs_1'}, dimensions={0}, use_global_device_ids=true | all-gather | bytes 202752 | tf_op jit(solution)/shard_map/all_gather | solution.py:43
  186.3 0.8 fusion.13
  187.1 0.8 fusion.12
  187.9 48.7 %all_gather.39 = bf16[2048,192]{1,0:T(8,128)(2,1)S(1)} all-gather(bf16[64,192]{1,0:T(8,128)(2,1)S(1)} %pad_maximum_fusion.1), channel_id=1, replica_groups=mesh['fs_0'=8,'fs_1'=4,'tp_0'=4,'tp_1'=2] {'fs_0','fs_1'}, dimensions={0}, use_global_device_ids=true | all-gather | bytes 811008 | tf_op jit(solution)/shard_map/all_gather | solution.py:43
  236.6 0.8 slice.18
  237.4 0.9 copy.27
  (46 shorter events, 4.4 us)
Async XLA Ops:
  0.6 20.4 %copy-start = (bf16[2560,128]{1,0:T(8,128)(2,1)S(1)}, bf16[2560,128]{1,0:T(8,128)(2,1)}, u32[]{:S(2)}) copy-start(bf16[2560,128]{1,0:T(8,128)(2,1)} %param.12) | copy-start | bytes 1966084
  7.8 38.5 %copy-start.1 = (bf16[64,256]{1,0:T(8,128)(2,1)S(1)}, bf16[64,256]{1,0:T(8,128)(2,1)}, u32[]{:S(2)}) copy-start(bf16[64,256]{1,0:T(8,128)(2,1)} %param.17) | copy-start | bytes 98308
  9.2 61.4 %copy-start.2 = (bf16[64,256]{1,0:T(8,128)(2,1)S(1)}, bf16[64,256]{1,0:T(8,128)(2,1)}, u32[]{:S(2)}) copy-start(bf16[64,256]{1,0:T(8,128)(2,1)} %param.16) | copy-start | bytes 98308
  9.2 28.6 %all-to-all-start.1 = ((f32[32,1,4096]{2,1,0:T(1,128)}), f32[32,1,4096]{2,1,0:T(1,128)S(1)}, u32[]{:S(2)}, u32[]{:S(2)}) async-start(f32[32,1,4096]{2,1,0:T(1,128)} %reshape.52), calls=%async_computation.1 | async-start | bytes 1048576 | tf_op jit(solution)/shard_map/all_to_all | solution.py:28
  21.0 56.4 %copy-start.12 = (u32[256]{0:T(256)S(1)}, u32[256]{0:T(256)}, u32[]{:S(2)}) copy-start(u32[256]{0:T(256)} %constant.36) | copy-start | bytes 3076
  21.0 66.4 %copy-start.5 = (f32[8,64]{1,0:T(8,128)S(1)}, f32[8,64]{1,0:T(8,128)}, u32[]{:S(2)}) copy-start(f32[8,64]{1,0:T(8,128)} %param.21) | copy-start | bytes 6148
  21.0 66.3 %copy-start.6 = (f32[8,64]{1,0:T(8,128)S(1)}, f32[8,64]{1,0:T(8,128)}, u32[]{:S(2)}) copy-start(f32[8,64]{1,0:T(8,128)} %param.20) | copy-start | bytes 6148
  21.0 67.5 %copy-start.7 = (f32[8,128]{1,0:T(8,128)S(1)}, f32[8,128]{1,0:T(8,128)}, u32[]{:S(2)}) copy-start(f32[8,128]{1,0:T(8,128)} %param.19) | copy-start | bytes 12292
  21.1 67.5 %copy-start.8 = (f32[8,128]{1,0:T(8,128)S(1)}, f32[8,128]{1,0:T(8,128)}, u32[]{:S(2)}) copy-start(f32[8,128]{1,0:T(8,128)} %param.18) | copy-start | bytes 12292
  21.1 70.8 %copy-start.11 = (u32[256]{0:T(256)S(1)}, u32[256]{0:T(256)}, u32[]{:S(2)}) copy-start(u32[256]{0:T(256)} %constant.41) | copy-start | bytes 3076
  21.1 88.8 %copy-start.10 = (u32[256]{0:T(256)S(1)}, u32[256]{0:T(256)}, u32[]{:S(2)}) copy-start(u32[256]{0:T(256)} %constant.46) | copy-start | bytes 3076
  21.1 100.8 %copy-start.9 = (u32[256]{0:T(256)S(1)}, u32[256]{0:T(256)}, u32[]{:S(2)}) copy-start(u32[256]{0:T(256)} %constant.51) | copy-start | bytes 3076
  21.1 165.1 %copy-start.3 = (f32[64,64]{1,0:T(8,128)S(1)}, f32[64,64]{1,0:T(8,128)}, u32[]{:S(2)}) copy-start(f32[64,64]{1,0:T(8,128)} %param.15) | copy-start | bytes 49156
  21.1 166.0 %copy-start.4 = (f32[64,128]{1,0:T(8,128)S(1)}, f32[64,128]{1,0:T(8,128)}, u32[]{:S(2)}) copy-start(f32[64,128]{1,0:T(8,128)} %param.14) | copy-start | bytes 98308
  37.8 32.8 %all-to-all-start = ((f32[32,64,128]{2,1,0:T(8,128)}), f32[32,64,128]{2,1,0:T(8,128)S(1)}, u32[]{:S(2)}, u32[]{:S(2)}) async-start(f32[32,64,128]{2,1,0:T(8,128)} %bitcast), calls=%async_computation | async-start | bytes 2097152 | tf_op jit(solution)/shard_map/all_to_all | solution.py:28
  71.8 15.5 %all-to-all-start.2 = ((f32[32,8,192]{2,1,0:T(8,128)}), f32[32,8,192]{2,1,0:T(8,128)S(1)}, u32[]{:S(2)}, u32[]{:S(2)}) async-start(f32[32,8,192]{2,1,0:T(8,128)} %bitcast.3), calls=%async_computation.2 | async-start | bytes 524288 | tf_op jit(solution)/shard_map/all_to_all | solution.py:28
